TPU v7x, 32 devices: a whole 2x2x4 slice. The times are simulated.
32 devices in a mesh: rep: 2 (over x), fs: 8 (over z, y), tp: 2 (over core).
Axes of the slice: x: 2, y: 2, z: 4, core: 2. Of those that a mesh axis runs over, the one named last changes fastest.
Arguments:
- pre_gate: bfloat16 [12288, 4096], P(('rep', 'fs'), 'tp'), may hold values from -6 to 6
- pre_linear: bfloat16 [12288, 4096], P(('rep', 'fs'), 'tp'), may hold values from -6 to 6
- taps_gate: float32 [3, 4096], P(None, 'tp'), may hold values from -3.5 to 3.5
- taps_linear: float32 [3, 4096], P(None, 'tp'), may hold values from -3.5 to 3.5
- bias_gate: float32 [4096], P('tp'), may hold values from -3 to 3
- bias_linear: float32 [4096], P('tp'), may hold values from -3 to 3
- down_weight: bfloat16 [4096, 2048], P('tp', 'fs'), may hold values from -0.09375 to 0.09375
- out_grad: bfloat16 [12288, 2048], P(('rep', 'fs')), may hold values from -8 to 8
Outputs:
- grad_gate: bfloat16 [12288, 4096], P(('rep', 'fs'), 'tp')
- grad_linear: bfloat16 [12288, 4096], P(('rep', 'fs'), 'tp')
- grad_taps_gate: float32 [3, 4096], P(None, 'tp')
- grad_taps_linear: float32 [3, 4096], P(None, 'tp')
- grad_bias_gate: float32 [4096], P('tp')
- grad_bias_linear: float32 [4096], P('tp')
- grad_down: float32 [4096, 2048], P('tp', 'fs')
- row_norms: float32 [4096], P('tp')
All inputs are finite; a program needn't handle non-finite values.
Results may differ from a plain program's by a relative error of at most 0.0031.
Values may be sent and summed in bfloat16 or wider, within the bound.
No kernel may reach another device: no remote copies, remote signals or barrier semaphores. Data moves between devices by JAX's collectives and lax.ppermute only.
A program may use at most 128 MiB of HBM per device.

v0:
```python
import jax
import jax.numpy as jnp
from jax import lax
from jax.sharding import PartitionSpec as P


def convolve(values, taps, bias):
    length = values.shape[0]
    padded = jnp.pad(values, ((2, 0), (0, 0)))
    return (
        taps[0] * padded[0:length]
        + taps[1] * padded[1 : length + 1]
        + taps[2] * padded[2 : length + 2]
        + bias
    )


def convolve_back(grads, taps):
    length = grads.shape[0]
    padded = jnp.pad(grads, ((0, 2), (0, 0)))
    return (
        taps[0] * padded[2 : length + 2]
        + taps[1] * padded[1 : length + 1]
        + taps[2] * padded[0:length]
    )


def tap_grads(grads, values):
    length = values.shape[0]
    padded = jnp.pad(values, ((2, 0), (0, 0)))
    return jnp.stack([jnp.sum(grads * padded[j : j + length], axis=0) for j in range(3)])


def local(
    pre_gate, pre_linear, taps_gate, taps_linear, bias_gate, bias_linear, down_weight, out_grad
):
    gate_in = pre_gate.astype(jnp.float32)
    linear_in = pre_linear.astype(jnp.float32)
    gate_pre = convolve(gate_in, taps_gate, bias_gate)
    linear_pre = convolve(linear_in, taps_linear, bias_linear)
    sigma = jax.nn.sigmoid(gate_pre)
    silu_val = gate_pre * sigma
    hidden = (silu_val * linear_pre).astype(jnp.bfloat16)
    columns = out_grad
    grad_hidden = lax.dot_general(
        columns,
        lax.all_gather(down_weight, "fs", axis=1, tiled=True),
        (((1,), (1,)), ((), ())),
        preferred_element_type=jnp.float32,
    )
    grad_gate_pre = grad_hidden * linear_pre * sigma * (1.0 + gate_pre * (1.0 - sigma))
    grad_linear_pre = grad_hidden * silu_val
    grad_gate = convolve_back(grad_gate_pre, taps_gate).astype(jnp.bfloat16)
    grad_linear = convolve_back(grad_linear_pre, taps_linear).astype(jnp.bfloat16)
    conv_parts = (
        tap_grads(grad_gate_pre, gate_in),
        tap_grads(grad_linear_pre, linear_in),
        jnp.sum(grad_gate_pre, axis=0),
        jnp.sum(grad_linear_pre, axis=0),
    )
    grad_taps_gate, grad_taps_linear, grad_bias_gate, grad_bias_linear = lax.psum(
        (conv_parts[0], conv_parts[1], conv_parts[2], conv_parts[3]), ("rep", "fs")
    )
    columns = out_grad
    partial_grad = lax.psum_scatter(
        lax.dot_general(
            columns, hidden, (((0,), (0,)), ((), ())), preferred_element_type=jnp.float32
        ),
        "fs",
        scatter_dimension=0,
        tiled=True,
    )
    summed = lax.psum(partial_grad, "rep")
    grad_down = summed.T
    row_norms = lax.psum(jnp.sum(grad_down * grad_down, axis=1), "fs")
    return (
        grad_gate,
        grad_linear,
        grad_taps_gate,
        grad_taps_linear,
        grad_bias_gate,
        grad_bias_linear,
        grad_down,
        row_norms,
    )


def solution(mesh):
    in_specs = (
        P(("rep", "fs"), "tp"),
        P(("rep", "fs"), "tp"),
        P(None, "tp"),
        P(None, "tp"),
        P("tp"),
        P("tp"),
        P("tp", "fs"),
        P(("rep", "fs"), None),
    )
    out_specs = (
        P(("rep", "fs"), "tp"),
        P(("rep", "fs"), "tp"),
        P(None, "tp"),
        P(None, "tp"),
        P("tp"),
        P("tp"),
        P("tp", "fs"),
        P("tp"),
    )
    return jax.shard_map(local, mesh=mesh, in_specs=in_specs, out_specs=out_specs, check_vma=False)
```

profile of v0, /device:TPU:0, one launch (start us, length us, event | category | flops | bytes accessed | tf_op | source)
XLA Modules:
  0.0 668.1 jit_solution(7865275278848254621)
XLA Ops:
  7.2 0.0 copy-start
  7.2 0.0 all-gather.2.cloned.1.call-start
  7.2 0.7 all-gather.2.cloned.1.call-update
  7.9 0.0 reduce-scatter.2.cloned.1.call-start
  8.0 0.0 copy-start.3
  8.0 5.6 convert_element_type.24
  13.5 0.0 copy-done.3
  13.5 0.0 copy-start.4
  13.5 0.0 copy-start.5
  13.5 0.0 copy-start.7
  13.5 3.4 convert_element_type.23
  17.0 0.0 copy-done.4
  17.0 0.0 copy-done.5
  17.0 120.7 %all-gather.2.cloned.1.call-done = bf16[2048,2048]{1,0:T(8,128)(2,1)} async-done(((bf16[2048,256]{1,0:T(8,128)(2,1)}), bf16[2048,2048]{1,0:T(8,128)(2,1)}) %all-gather.2.cloned.1.call-update) | async-done | bytes 8388624 | tf_op jit(solution)/shard_map/all_gather | solution.py:47
  137.7 0.0 copy-done
  137.7 0.0 copy-done.7
  137.7 0.0 copy-start.1
  137.7 0.0 copy-start.2
  137.7 0.0 copy-start.6
  137.8 25.9 %fusion.4 = (f32[2048]{0:T(1024)}, f32[2048]{0:T(1024)S(1)}, f32[2048]{0:T(1024)S(1)}, f32[2048]{0:T(1024)S(1)}, f32[768,2048]{1,0:T(8,128)}, /*index=5*/f32[768,2048]{1,0:T(8,128)}, f32[768,2048]{1,0:T(8,128)}) fusion(bf16[768,2048]{1,0:T(8,128)(2,1)} %param.9, f32[768,2048]{1,0:T(8,128)} %convert_element_type.23, f32[2048]{0:T(1024)S(1)} %copy-done.7, ...), kind=kOutput, calls=%fused_computation.24 | convolution fusion | flops 6472327168 | bytes 46202880 | tf_op jit(solution)/shard_map/dot_general | solution.py:45
  163.7 0.0 copy-done.1
  163.7 0.0 copy-done.2
  163.7 0.0 copy-done.6
  163.7 19.0 %fusion.5 = (f32[2048]{0:T(1024)}, f32[2048]{0:T(1024)S(1)}, f32[2048]{0:T(1024)S(1)}, f32[2048]{0:T(1024)S(1)}, f32[768,2048]{1,0:T(8,128)}, /*index=5*/f32[768,2048]{1,0:T(8,128)}, bf16[768,2048]{1,0:T(8,128)(2,1)}) fusion(bf16[768,2048]{1,0:T(8,128)(2,1)} %param.8, f32[768,2048]{1,0:T(8,128)S(1)} %copy-done.1, f32[768,2048]{1,0:T(8,128)} %get-tuple-element.25, ...), kind=kLoop, calls=%fused_computation.25 | loop fusion | flops 45604864 | bytes 50397184 | tf_op jit(solution)/shard_map/reduce_sum | solution.py:58
  182.7 15.2 %convolution_bitcast_fusion = f32[2048,2048]{0,1:T(8,128)} fusion(bf16[768,2048]{1,0:T(8,128)(2,1)S(1)} %copy-done, f32[768,2048]{1,0:T(8,128)} %get-tuple-element.27, f32[768,2048]{1,0:T(8,128)} %get-tuple-element.25), kind=kOutput, calls=%fused_computation | convolution fusion | flops 6451888128 | bytes 32505856 | tf_op jit(solution)/shard_map/dot_general | solution.py:66
  197.8 0.0 reduce-scatter.2.cloned.1.call-update
  197.9 0.0 all-reduce.8.cloned.1.call-start
  197.9 278.5 %reduce-scatter.2.cloned.1.call-done = f32[256,2048]{0,1:T(8,128)} async-done(((f32[2048,2048]{0,1:T(8,128)}), f32[256,2048]{0,1:T(8,128)}) %reduce-scatter.2.cloned.1.call-update) | async-done | bytes 2097168 | tf_op jit(solution)/shard_map/reduce_scatter | solution.py:65
  476.4 0.0 all-reduce.8.cloned.1.call-update
  476.5 0.0 all-reduce.10.cloned.1.call-start
  476.5 0.7 pad_maximum_fusion
  477.2 9.6 %add_convert_fusion.1 = bf16[768,2048]{1,0:T(8,128)(2,1)} fusion(f32[768,2048]{1,0:T(8,128)} %get-tuple-element.26, f32[2048]{0:T(1024)S(1)} %bitcast.28, f32[2048]{0:T(1024)S(1)} %bitcast.30, f32[2048]{0:T(1024)S(1)} %bitcast.26), kind=kLoop, calls=%fused_computation.9 | loop fusion | flops 9437184 | bytes 9461760 | tf_op jit(solution)/shard_map/convert_element_type | solution.py:53
  486.8 0.0 all-reduce.10.cloned.1.call-update
  486.8 54.0 %all-reduce.8.cloned.1.call-done = f32[2048,256]{1,0:T(8,128)} async-done(((f32[2048,256]{1,0:T(8,128)}), f32[2048,256]{1,0:T(8,128)}) %all-reduce.8.cloned.1.call-update) | async-done | bytes 2097168 | tf_op jit(solution)/shard_map/psum | solution.py:73
  540.8 1.9 multiply_reduce_fusion.6
  542.8 22.3 %psum.47 = f32[2048]{0:T(1024)} all-reduce(f32[2048]{0:T(1024)S(1)} %multiply_reduce_fusion.6), channel_id=1, replica_groups=mesh['rep'=2,'fs'=8,'tp'=2] {'fs'}, use_global_device_ids=true, to_apply=%region_15.16 | all-reduce | flops 2048 | bytes 16384 | tf_op jit(solution)/shard_map/psum | solution.py:75
  565.1 88.1 %all-reduce.10.cloned.1.call-done = (f32[3,2048]{1,0:T(4,128)}, f32[3,2048]{1,0:T(4,128)}, f32[2048]{0:T(1024)}, f32[2048]{0:T(1024)}) async-done(((f32[3,2048]{1,0:T(4,128)}, f32[3,2048]{1,0:T(4,128)}, f32[2048]{0:T(1024)}, f32[2048]{0:T(1024)}), (f32[3,2048]{1,0:T(4,128)}, f32[3,2048]{1,0:T(4,128)}, f32[2048]{0:T(1024)}, f32[2048]{0:T(1024)})) %all-reduce.10.cloned.1.call-update) | async-done | bytes 65552 | tf_op jit(solution)/shard_map/psum | solution.py:61
  653.2 1.4 copy.21
  654.6 1.4 copy.22
  655.9 1.3 copy.23
  657.2 1.3 copy.24
  658.5 3.0 copy.25
  (2 shorter events, 0.0 us)
Async XLA Ops:
  7.2 130.6 %copy-start = (bf16[768,2048]{1,0:T(8,128)(2,1)S(1)}, bf16[768,2048]{1,0:T(8,128)(2,1)}, u32[]{:S(2)}) copy-start(bf16[768,2048]{1,0:T(8,128)(2,1)} %param.15) | copy-start | bytes 9437188
  7.2 130.5 %all-gather.2.cloned.1.call-start = ((), (), s32[]{:S(2)}) async-start(), calls=%async_computation.1 | async-start | bytes 9437184 | tf_op jit(solution)/shard_map/all_gather | solution.py:47
  7.9 468.5 %reduce-scatter.2.cloned.1.call-start = ((), (), s32[]{:S(2)}) async-start(), calls=%async_computation.2 | async-start | bytes 18874368 | tf_op jit(solution)/shard_map/reduce_scatter | solution.py:65
  8.0 5.6 copy-start.3
  13.5 3.4 copy-start.4
  13.5 3.5 copy-start.5
  13.5 124.2 %copy-start.7 = (f32[2048]{0:T(1024)S(1)}, f32[2048]{0:T(1024)}, u32[]{:S(2)}) copy-start(f32[2048]{0:T(1024)} %param.12) | copy-start | bytes 24580
  137.7 25.9 %copy-start.1 = (f32[768,2048]{1,0:T(8,128)S(1)}, f32[768,2048]{1,0:T(8,128)}, u32[]{:S(2)}) copy-start(f32[768,2048]{1,0:T(8,128)} %convert_element_type.24) | copy-start | bytes 18874372
  137.7 25.9 %copy-start.2 = (f32[768,2048]{1,0:T(8,128)S(1)}, f32[768,2048]{1,0:T(8,128)}, u32[]{:S(2)}) copy-start(f32[768,2048]{1,0:T(8,128)} %convert_element_type.23) | copy-start | bytes 18874372
  137.7 25.9 %copy-start.6 = (f32[2048]{0:T(1024)S(1)}, f32[2048]{0:T(1024)}, u32[]{:S(2)}) copy-start(f32[2048]{0:T(1024)} %param.13) | copy-start | bytes 24580
  197.9 343.0 %all-reduce.8.cloned.1.call-start = ((), (), s32[]{:S(2)}) async-start(), calls=%async_computation.3 | async-start | bytes 4194304 | tf_op jit(solution)/shard_map/psum | solution.py:73
  476.5 176.7 %all-reduce.10.cloned.1.call-start = ((), (), s32[]{:S(2)}) async-start(), calls=%async_computation.4 | async-start | bytes 163840 | tf_op jit(solution)/shard_map/psum | solution.py:61
Sparse Core Ops, SparseCore 0:
  10.0 127.6 all-gather.1
  198.0 278.3 reduce-scatter.1
  478.7 62.0 all-reduce.7
  547.2 105.9 all-reduce.9
where the time goes:
time: 669 us; the launch traced here: 668 us
  waiting for transfers between devices  542 us (81%)
  matrix products  41.1 us (6%)
  other arithmetic  40.2 us (6%)
  blocking collectives  22.3 us (3%)
  between operations  13.8 us (2%)
  local copies, waits for them, and re-layouts  8.47 us (1%)
    reduce_scatter x1, waiting for transfers between devices, local(): lax.psum_scatter(lax.dot_general(columns, hidden, (((0,), (0,)), ((), ())...  279 us
    all_gather x1, waiting for transfers between devices, local(): lax.all_gather(down_weight, 'fs', axis=1, tiled=True)  121 us
    psum x1, waiting for transfers between devices, local(): lax.psum((conv_parts[0], conv_parts[1], conv_parts[2], conv_parts[3]), ('...  88.1 us
    psum x1, waiting for transfers between devices, local(): summed = lax.psum(partial_grad, 'rep')  54 us
    dot_general x1, matrix products, local(): lax.dot_general(columns, lax.all_gather(down_weight, 'fs', axis=1, tiled=...  25.9 us
    psum x1, blocking collectives, local(): row_norms = lax.psum(jnp.sum(grad_down * grad_down, axis=1), 'fs')  22.3 us
    reduce_sum x1, other arithmetic, local(): jnp.sum(grad_gate_pre, axis=0)  19 us
    dot_general x1, matrix products, local(): lax.dot_general(columns, hidden, (((0,), (0,)), ((), ())), preferred_elem...  15.2 us
  transfers between devices with their start and end apart: 4, of which 4 were waited for; matrix products, arithmetic and copies ran while one was open for 3% of the time, Pallas kernels for 0%

commit v1 on v0

--- a/solution.py
+++ b/solution.py
@@ -59,7 +59,7 @@
         jnp.sum(grad_linear_pre, axis=0),
     )
     grad_taps_gate, grad_taps_linear, grad_bias_gate, grad_bias_linear = lax.psum(
-        (conv_parts[0], conv_parts[1], conv_parts[2], conv_parts[3]), ("rep", "fs")
+        lax.psum((conv_parts[0], conv_parts[1], conv_parts[2], conv_parts[3]), "rep"), "fs"
     )
     columns = out_grad
     partial_grad = lax.psum_scatter(

time: 669 us -> 658 us (0.984)
  blocking collectives: 22.3 us -> 0 us
  waiting for transfers between devices: 542 us -> 551 us
    psum x1 -> x0, blocking collectives: 22.3 us -> none  [local(): row_norms = lax.psum(jnp.sum(grad_down * grad_down, axis=1), 'fs')]
    psum x1, waiting for transfers between devices: 54 us -> 63.6 us  [local(): summed = lax.psum(partial_grad, 'rep')]
    psum x1 -> x2, waiting for transfers between devices: 88.1 us -> 87.8 us  [the longest x1 66.3 us: local(): lax.psum(lax.psum((conv_parts[0], conv_parts[1], conv_parts[2], conv_part...]
  transfers between devices with their start and end apart: 4 -> 5, of which waited for: 4 -> 5; matrix products, arithmetic and copies ran while one was open for 3% -> 3% of each run, Pallas kernels for 0% -> 0%
where the time goes in v1:
time: 658 us; the launch traced here: 657 us
  waiting for transfers between devices  551 us (84%)
  matrix products  41.1 us (6%)
  other arithmetic  41 us (6%)
  between operations  13.8 us (2%)
  local copies, waits for them, and re-layouts  9.76 us (1%)
    reduce_scatter x1, waiting for transfers between devices, local(): lax.psum_scatter(lax.dot_general(columns, hidden, (((0,), (0,)), ((), ())...  279 us
    all_gather x1, waiting for transfers between devices, local(): lax.all_gather(down_weight, 'fs', axis=1, tiled=True)  121 us
    psum x1, waiting for transfers between devices, local(): lax.psum(lax.psum((conv_parts[0], conv_parts[1], conv_parts[2], conv_part...  66.3 us
    psum x1, waiting for transfers between devices, local(): summed = lax.psum(partial_grad, 'rep')  63.6 us
    dot_general x1, matrix products, local(): lax.dot_general(columns, lax.all_gather(down_weight, 'fs', axis=1, tiled=...  25.9 us
    psum x1, waiting for transfers between devices, local(): lax.psum((conv_parts[0], conv_parts[1], conv_parts[2], conv_parts[3]), 'r...  21.5 us
    reduce_sum x1, other arithmetic, local(): jnp.sum(grad_gate_pre, axis=0)  19.5 us
    dot_general x1, matrix products, local(): lax.dot_general(columns, hidden, (((0,), (0,)), ((), ())), preferred_elem...  15.2 us
  transfers between devices with their start and end apart: 5, of which 5 were waited for; matrix products, arithmetic and copies ran while one was open for 3% of the time, Pallas kernels for 0%

profile of v1, /device:TPU:0, one launch (start us, length us, event | category | flops | bytes accessed | tf_op | source)
XLA Modules:
  0.0 657.4 jit_solution(4270742734075744472)
XLA Ops:
  7.2 0.0 copy-start
  7.2 0.0 all-gather.2.cloned.1.call-start
  7.2 0.7 all-gather.2.cloned.1.call-update
  7.9 0.0 reduce-scatter.2.cloned.1.call-start
  8.0 0.0 copy-start.3
  8.0 5.5 convert_element_type.24
  13.4 0.0 copy-done.3
  13.4 0.0 copy-start.4
  13.4 0.0 copy-start.5
  13.4 0.0 copy-start.7
  13.5 3.4 convert_element_type.23
  16.9 0.0 copy-done.4
  16.9 0.0 copy-done.5
  16.9 120.8 %all-gather.2.cloned.1.call-done = bf16[2048,2048]{1,0:T(8,128)(2,1)} async-done(((bf16[2048,256]{1,0:T(8,128)(2,1)}), bf16[2048,2048]{1,0:T(8,128)(2,1)}) %all-gather.2.cloned.1.call-update) | async-done | bytes 8388624 | tf_op jit(solution)/shard_map/all_gather | solution.py:47
  137.7 0.0 copy-done
  137.7 0.0 copy-done.7
  137.7 0.0 copy-start.1
  137.7 0.0 copy-start.2
  137.7 0.0 copy-start.6
  137.8 25.9 %fusion.4 = (f32[2048]{0:T(1024)}, f32[2048]{0:T(1024)S(1)}, f32[2048]{0:T(1024)S(1)}, f32[2048]{0:T(1024)S(1)}, f32[768,2048]{1,0:T(8,128)}, /*index=5*/f32[768,2048]{1,0:T(8,128)}, f32[768,2048]{1,0:T(8,128)}) fusion(bf16[768,2048]{1,0:T(8,128)(2,1)} %param.9, f32[768,2048]{1,0:T(8,128)} %convert_element_type.23, f32[2048]{0:T(1024)S(1)} %copy-done.7, ...), kind=kOutput, calls=%fused_computation.24 | convolution fusion | flops 6472327168 | bytes 46202880 | tf_op jit(solution)/shard_map/dot_general | solution.py:45
  163.7 0.0 copy-done.1
  163.7 0.0 copy-done.2
  163.7 0.0 copy-done.6
  163.7 19.5 %fusion.5 = (f32[2048]{0:T(1024)}, f32[2048]{0:T(1024)S(1)}, f32[2048]{0:T(1024)S(1)}, f32[2048]{0:T(1024)S(1)}, f32[768,2048]{1,0:T(8,128)}, /*index=5*/f32[768,2048]{1,0:T(8,128)}, bf16[768,2048]{1,0:T(8,128)(2,1)}) fusion(bf16[768,2048]{1,0:T(8,128)(2,1)} %param.8, f32[768,2048]{1,0:T(8,128)S(1)} %copy-done.1, f32[768,2048]{1,0:T(8,128)} %get-tuple-element.30, ...), kind=kLoop, calls=%fused_computation.25 | loop fusion | flops 45604864 | bytes 50397184 | tf_op jit(solution)/shard_map/reduce_sum | solution.py:58
  183.2 15.2 %convolution_bitcast_fusion = f32[2048,2048]{0,1:T(8,128)} fusion(bf16[768,2048]{1,0:T(8,128)(2,1)S(1)} %copy-done, f32[768,2048]{1,0:T(8,128)} %get-tuple-element.32, f32[768,2048]{1,0:T(8,128)} %get-tuple-element.30), kind=kOutput, calls=%fused_computation | convolution fusion | flops 6451888128 | bytes 32505856 | tf_op jit(solution)/shard_map/dot_general | solution.py:66
  198.3 0.0 reduce-scatter.2.cloned.1.call-update
  198.4 0.0 all-reduce.10.cloned.1.call-start
  198.4 278.5 %reduce-scatter.2.cloned.1.call-done = f32[256,2048]{0,1:T(8,128)} async-done(((f32[2048,2048]{0,1:T(8,128)}), f32[256,2048]{0,1:T(8,128)}) %reduce-scatter.2.cloned.1.call-update) | async-done | bytes 2097168 | tf_op jit(solution)/shard_map/reduce_scatter | solution.py:65
  476.9 0.0 all-reduce.10.cloned.1.call-update
  476.9 0.0 all-reduce.14.cloned.1.call-start
  477.0 0.7 pad_maximum_fusion
  477.7 0.0 all-reduce.14.cloned.1.call-update
  477.7 0.0 all-reduce.12.cloned.1.call-start
  477.7 63.6 %all-reduce.10.cloned.1.call-done = f32[2048,256]{1,0:T(8,128)} async-done(((f32[2048,256]{1,0:T(8,128)}), f32[2048,256]{1,0:T(8,128)}) %all-reduce.10.cloned.1.call-update) | async-done | bytes 2097168 | tf_op jit(solution)/shard_map/psum | solution.py:73
  541.3 2.5 multiply_reduce_fusion.6
  543.9 21.5 %all-reduce.14.cloned.1.call-done = (f32[3,2048]{1,0:T(4,128)}, f32[3,2048]{1,0:T(4,128)}, f32[2048]{0:T(1024)}, f32[2048]{0:T(1024)}) async-done(((f32[3,2048]{1,0:T(4,128)}, f32[3,2048]{1,0:T(4,128)}, f32[2048]{0:T(1024)}, f32[2048]{0:T(1024)}), (f32[3,2048]{1,0:T(4,128)}, f32[3,2048]{1,0:T(4,128)}, f32[2048]{0:T(1024)}, f32[2048]{0:T(1024)})) %all-reduce.14.cloned.1.call-update) | async-done | bytes 65552 | tf_op jit(solution)/shard_map/psum | solution.py:62
  565.4 0.0 all-reduce.12.cloned.1.call-update
  565.4 9.4 %add_convert_fusion.1 = bf16[768,2048]{1,0:T(8,128)(2,1)} fusion(f32[768,2048]{1,0:T(8,128)} %get-tuple-element.31, f32[2048]{0:T(1024)S(1)} %bitcast.28, f32[2048]{0:T(1024)S(1)} %bitcast.30, f32[2048]{0:T(1024)S(1)} %bitcast.26), kind=kLoop, calls=%fused_computation.9 | loop fusion | flops 9437184 | bytes 9461760 | tf_op jit(solution)/shard_map/convert_element_type | solution.py:53
  574.8 66.3 %all-reduce.12.cloned.1.call-done = (f32[3,2048]{1,0:T(4,128)}, f32[3,2048]{1,0:T(4,128)}, f32[2048]{0:T(1024)}, f32[2048]{0:T(1024)}, f32[2048]{0:T(1024)}) async-done(((f32[3,2048]{1,0:T(4,128)}, f32[3,2048]{1,0:T(4,128)}, f32[2048]{0:T(1024)}, f32[2048]{0:T(1024)}, f32[2048]{0:T(1024)}), (f32[3,2048]{1,0:T(4,128)}, f32[3,2048]{1,0:T(4,128)}, f32[2048]{0:T(1024)}, f32[2048]{0:T(1024)}, ...) | async-done | bytes 73744 | tf_op jit(solution)/shard_map/psum | solution.py:61
  641.2 1.4 copy.26
  642.5 1.4 copy.27
  643.9 1.3 copy.28
  645.2 1.3 copy.29
  646.5 3.0 copy.30
  649.5 1.3 copy.31
  (2 shorter events, 0.0 us)
Async XLA Ops:
  7.2 130.6 %copy-start = (bf16[768,2048]{1,0:T(8,128)(2,1)S(1)}, bf16[768,2048]{1,0:T(8,128)(2,1)}, u32[]{:S(2)}) copy-start(bf16[768,2048]{1,0:T(8,128)(2,1)} %param.15) | copy-start | bytes 9437188
  7.2 130.5 %all-gather.2.cloned.1.call-start = ((), (), s32[]{:S(2)}) async-start(), calls=%async_computation.1 | async-start | bytes 9437184 | tf_op jit(solution)/shard_map/all_gather | solution.py:47
  7.9 469.0 %reduce-scatter.2.cloned.1.call-start = ((), (), s32[]{:S(2)}) async-start(), calls=%async_computation.2 | async-start | bytes 18874368 | tf_op jit(solution)/shard_map/reduce_scatter | solution.py:65
  8.0 5.5 copy-start.3
  13.4 3.4 copy-start.4
  13.4 3.5 copy-start.5
  13.4 124.3 %copy-start.7 = (f32[2048]{0:T(1024)S(1)}, f32[2048]{0:T(1024)}, u32[]{:S(2)}) copy-start(f32[2048]{0:T(1024)} %param.12) | copy-start | bytes 24580
  137.7 25.9 %copy-start.1 = (f32[768,2048]{1,0:T(8,128)S(1)}, f32[768,2048]{1,0:T(8,128)}, u32[]{:S(2)}) copy-start(f32[768,2048]{1,0:T(8,128)} %convert_element_type.24) | copy-start | bytes 18874372
  137.7 25.9 %copy-start.2 = (f32[768,2048]{1,0:T(8,128)S(1)}, f32[768,2048]{1,0:T(8,128)}, u32[]{:S(2)}) copy-start(f32[768,2048]{1,0:T(8,128)} %convert_element_type.23) | copy-start | bytes 18874372
  137.7 25.9 %copy-start.6 = (f32[2048]{0:T(1024)S(1)}, f32[2048]{0:T(1024)}, u32[]{:S(2)}) copy-start(f32[2048]{0:T(1024)} %param.13) | copy-start | bytes 24580
  198.4 343.0 %all-reduce.10.cloned.1.call-start = ((), (), s32[]{:S(2)}) async-start(), calls=%async_computation.3 | async-start | bytes 4194304 | tf_op jit(solution)/shard_map/psum | solution.py:73
  476.9 88.4 %all-reduce.14.cloned.1.call-start = ((), (), s32[]{:S(2)}) async-start(), calls=%async_computation.5 | async-start | bytes 163840 | tf_op jit(solution)/shard_map/psum | solution.py:62
  477.7 163.5 %all-reduce.12.cloned.1.call-start = ((), (), s32[]{:S(2)}) async-start(), calls=%async_computation.4 | async-start | bytes 180224 | tf_op jit(solution)/shard_map/psum | solution.py:61
Sparse Core Ops, SparseCore 0:
  10.0 127.6 all-gather.1
  198.5 278.3 reduce-scatter.1
  479.2 62.0 all-reduce.9
  544.2 21.1 all-reduce.13
  569.7 71.3 all-reduce.11
